TPU v7x, 32 devices: a whole 2x2x4 slice. The times are simulated.
32 devices in a mesh: sp: 8 (over z, x), tp: 4 (over y, core).
Axes of the slice: x: 2, y: 2, z: 4, core: 2. Of those that a mesh axis runs over, the one named last changes fastest.
Arguments:
- queries: bfloat16 [8192, 1024], P('sp', 'tp'), may hold values from -75 to 75
- key_rows: bfloat16 [8192, 1024], P('sp', 'tp'), may hold values from -4 to 4
- value_rows: bfloat16 [8192, 1024], P('sp', 'tp'), may hold values from -6 to 6
- cum_gate: float32 [16, 8192], P('tp'), may hold values from -1172 to 0, as said below
- residual: bfloat16 [8192, 2048], P(('sp', 'tp')), may hold values from -6 to 6
- out_weight: bfloat16 [1024, 2048], replicated, may hold values from -0.1875 to 0.1875
- gain_mix: float32 [2048], replicated, may hold values from 0.1 to 1.9
- gain_pre: float32 [2048], replicated, may hold values from 0.1 to 1.9
- gain_post: float32 [2048], replicated, may hold values from 0.1 to 1.9
- route_ids: int32 [8192, 2], P(('sp', 'tp')), may hold values from 0 to 31, all different within a row; in each aligned block of 256 rows (0 to 255, 256 to 511, ...) at most 22 rows name the same one
- route_weight: float32 [8192, 2], P(('sp', 'tp')), may hold values from 0.2 to 1
- w_gate: bfloat16 [32, 2048, 512], P(('sp', 'tp')), may hold values from -0.125 to 0.125
- w_up: bfloat16 [32, 2048, 512], P(('sp', 'tp')), may hold values from -0.125 to 0.125
- w_down: bfloat16 [32, 512, 2048], P(('sp', 'tp')), may hold values from -0.25 to 0.25
Outputs:
- layer_out: bfloat16 [8192, 2048], P(('sp', 'tp'))
Inputs may be any that keep to these rules, and one draw needn't show every extreme that they name: `route_ids`: each row names 2 different experts; in the rows of one device no expert is named more than 22 times, a bound that some block reaches. `cum_gate`: along the positions each head's values never rise.
All inputs are finite; a program needn't handle non-finite values.
Results may differ from a plain program's by a relative error of at most 0.018.
Values may be sent and summed in bfloat16 or wider, within the bound.
A program may use at most 128 MiB of HBM per device.

v0:
```python
import math

import jax
import jax.numpy as jnp
from jax import lax
from jax.sharding import PartitionSpec as P

HEAD_DIM = 64


NORM_EPS = 1e-06
MASKED = -1e30


def rms_scale(rows, gain):
    mean_sq = jnp.mean(rows * rows, axis=-1, keepdims=True)
    return rows * lax.rsqrt(mean_sq + NORM_EPS) * gain


def attend(running, queries, gate_q, q_start, key_part, value_part, gate_k, k_start):
    row_peak, row_total, weighted = running
    scores = jnp.einsum(
        "qhd,khd->hqk", queries, key_part, preferred_element_type=jnp.float32
    ) * HEAD_DIM ** (-0.5)
    scores = scores + gate_q[:, :, None] - gate_k[:, None, :]
    query_pos = q_start + lax.iota(jnp.int32, queries.shape[0])
    key_pos = k_start + lax.iota(jnp.int32, key_part.shape[0])
    allowed = (key_pos[None, :] <= query_pos[:, None])[None]
    scores = jnp.where(allowed, scores, MASKED)
    new_peak = jnp.maximum(row_peak, jnp.max(scores, axis=-1))
    unnorm = jnp.where(allowed, jnp.exp(scores - new_peak[..., None]), 0.0)
    rescale = jnp.exp(row_peak - new_peak)
    row_total = row_total * rescale + jnp.sum(unnorm, axis=-1)
    weighted = weighted * rescale.T[:, :, None] + jnp.einsum(
        "hqk,khd->qhd", unnorm.astype(jnp.bfloat16), value_part, preferred_element_type=jnp.float32
    )
    return (new_peak, row_total, weighted)


def local(
    queries,
    key_rows,
    value_rows,
    cum_gate,
    residual,
    out_weight,
    gain_mix,
    gain_pre,
    gain_post,
    route_ids,
    route_weight,
    w_gate,
    w_up,
    w_down,
):
    tok_dev, feature_width = queries.shape
    local_heads = feature_width // HEAD_DIM
    my_start = lax.axis_index("sp") * tok_dev
    query_heads = queries.reshape(tok_dev, local_heads, HEAD_DIM)
    gate_q = lax.dynamic_slice_in_dim(cum_gate, my_start, tok_dev, 1)
    initial = (
        jnp.full((local_heads, tok_dev), MASKED, jnp.float32),
        jnp.zeros((local_heads, tok_dev), jnp.float32),
        jnp.zeros((tok_dev, local_heads, HEAD_DIM), jnp.float32),
    )
    paired = jnp.stack((key_rows, value_rows))

    def consume(running, key_part, value_part, k_start):
        row_count = key_part.shape[0]
        gate_k = lax.dynamic_slice_in_dim(cum_gate, k_start, row_count, 1)
        return attend(
            running,
            query_heads,
            gate_q,
            my_start,
            key_part.reshape(row_count, local_heads, HEAD_DIM),
            value_part.reshape(row_count, local_heads, HEAD_DIM),
            gate_k,
            k_start,
        )

    running = initial
    piece = lax.all_gather(paired, "sp", axis=1, tiled=True)
    row_count = piece.shape[1]
    span_rows = math.gcd(row_count, tok_dev)

    def single(block_index, running):
        offset = block_index * span_rows
        part = lax.dynamic_slice_in_dim(piece, offset, span_rows, 1)
        return lax.cond(
            offset < my_start + tok_dev,
            lambda state_now: consume(state_now, part[0], part[1], offset),
            lambda state_now: state_now,
            running,
        )

    running = lax.fori_loop(0, row_count // span_rows, single, running)
    row_peak, row_total, weighted = running
    attended = (
        (weighted / row_total.T[:, :, None]).astype(jnp.bfloat16).reshape(tok_dev, feature_width)
    )
    head_rows = lax.all_to_all(attended, "tp", split_axis=0, concat_axis=1, tiled=True)
    projected = jnp.dot(head_rows, out_weight, preferred_element_type=jnp.float32)
    stream = (residual.astype(jnp.float32) + rms_scale(projected, gain_mix)).astype(jnp.bfloat16)
    stream_wide = lax.optimization_barrier(stream).astype(jnp.float32)
    normed = rms_scale(stream_wide, gain_pre).astype(jnp.bfloat16)
    rows_dev, top_count = route_ids.shape
    model_width = normed.shape[1]
    experts_all = lax.axis_size("sp") * lax.axis_size("tp")
    capacity = max(2, (4 * rows_dev * top_count + 3 * experts_all - 1) // (3 * experts_all))
    flat_ids = route_ids.reshape(-1)
    onehot = (flat_ids[:, None] == lax.iota(jnp.int32, experts_all)[None, :]).astype(jnp.int32)
    slot_rank = jnp.sum(jnp.cumsum(onehot, axis=0) * onehot, axis=1) - 1
    slot_index = flat_ids * capacity + slot_rank
    spread = jnp.repeat(normed, top_count, axis=0)
    outgoing = (
        jnp.zeros((experts_all * capacity, model_width), jnp.bfloat16).at[slot_index].set(spread)
    )
    outgoing = outgoing.reshape(experts_all, capacity, model_width)
    arrived = lax.all_to_all(outgoing, ("sp", "tp"), split_axis=0, concat_axis=0, tiled=True)
    sources, slots, width_here = arrived.shape
    flat_rows = arrived.reshape(sources * slots, width_here)
    gate_act = jnp.dot(flat_rows, w_gate[0], preferred_element_type=jnp.float32)
    up_act = jnp.dot(flat_rows, w_up[0], preferred_element_type=jnp.float32)
    hidden = (jax.nn.silu(gate_act) * up_act).astype(jnp.bfloat16)
    expert_out = jnp.dot(hidden, w_down[0], preferred_element_type=jnp.float32).astype(jnp.bfloat16)
    returned = lax.all_to_all(
        expert_out.reshape(sources, slots, width_here),
        ("sp", "tp"),
        split_axis=0,
        concat_axis=0,
        tiled=True,
    )
    picked = returned.reshape(experts_all * capacity, model_width)[slot_index]
    picked = picked.reshape(rows_dev, top_count, model_width).astype(jnp.float32)
    combined = jnp.sum(picked * route_weight[:, :, None], axis=1)
    return (stream_wide + rms_scale(combined, gain_post)).astype(jnp.bfloat16)


def solution(mesh):
    return jax.shard_map(
        local,
        mesh=mesh,
        in_specs=(
            P("sp", "tp"),
            P("sp", "tp"),
            P("sp", "tp"),
            P("tp", None),
            P(("sp", "tp"), None),
            P(),
            P(),
            P(),
            P(),
            P(("sp", "tp"), None),
            P(("sp", "tp"), None),
            P(("sp", "tp"), None, None),
            P(("sp", "tp"), None, None),
            P(("sp", "tp"), None, None),
        ),
        out_specs=P(("sp", "tp"), None),
        check_vma=False,
    )
```

profile of v0, /device:TPU:0, one launch (start us, length us, event | category | flops | bytes accessed | tf_op | source)
XLA Modules:
  0.0 596.5 jit_solution(10661416319913627141)
XLA Ops:
  6.5 0.0 copy-start
  6.5 0.0 all-gather.2.cloned.1.call-start
  6.5 1.4 copy.40
  8.0 1.2 copy.41
  9.2 1.1 pad_maximum_fusion
  10.3 0.0 all-gather.2.cloned.1.call-update
  10.3 0.0 copy-done.7
  10.3 0.1 copy.45
  10.5 0.1 eq.29
  10.6 0.1 eq.25
  10.7 2.1 copy.42
  12.9 1.2 reduce-window.6
  14.0 0.2 slice_reduce_fusion
  14.3 0.1 copy.44
  14.4 0.2 mul.133
  14.6 0.7 constant_dynamic-slice_fusion.3
  15.3 0.1 fusion.33
  15.4 122.2 %all-gather.2.cloned.1.call-done = bf16[2,8192,256]{1,2,0:T(8,128)(2,1)} async-done(((bf16[2,1024,256]{1,2,0:T(8,128)(2,1)}), bf16[2,8192,256]{1,2,0:T(8,128)(2,1)}) %all-gather.2.cloned.1.call-update) | async-done | bytes 8388624 | tf_op jit(solution)/shard_map/all_gather | solution.py:83
  137.6 1.1 broadcast_in_dim.60
  138.7 27.2 %while.18 = (s32[]{:T(128)}, f32[4,1024]{1,0:T(4,128)S(1)}, f32[4,1024]{1,0:T(4,128)S(1)}, f32[1024,4,64]{0,2,1:T(8,128)}, s32[]{:T(128)}, /*index=5*/s32[]{:T(1...) while((s32[]{:T(128)}, f32[4,1024]{1,0:T(4,128)S(1)}, ...), condition=%wide.region_5.6_spmd, body=%wide.region_0.5_spmd.sunk | while | flops 1121466368 | bytes 129843592 | solution.py:97
  138.7 26.9 %conditional.2 = ((f32[4,1024]{1,0:T(4,128)S(1)}, f32[4,1024]{1,0:T(4,128)S(1)}, f32[1024,4,64]{0,2,1:T(8,128)})) conditional(s32[]{:T(128)} %convert_element_type.88, (f32[4,1024]{1,0:T(4,128)S(1)}, f32[4,1024]{1,0:T(4,128)S(1)}, f32[1024,4,64]{0,2,1:T(8,128)}) %tuple.52, (s32[]{:T(128)}, s32[]{:T(128)}, bf16[2,8192,256]{1,2,0:T(8,128)(2,1)}, ...), branch_computations={%region_1.0_spmd, %region_2.4_spmd} | conditional | flops 1121466368 | bytes 129843352 | solution.py:90
  138.7 0.0 copy-start.3
  138.8 1.3 constant_dynamic-slice_fusion.2
  140.1 0.7 broadcast_compare_fusion
  140.8 0.7 constant_dynamic-slice_fusion.1
  141.5 0.0 copy-done.3
  141.5 4.4 fusion.36
  145.9 0.0 copy-start.1
  145.9 5.7 copy-done.1
  151.6 5.2 fusion.8
  156.8 8.8 %fusion.1 = f32[4,1024]{1,0:T(4,128)S(1)} fusion(f32[4,1024,1024]{1,2,0:T(8,128)} %copy-done.1, f32[4,1024]{1,0:T(4,128)S(1)} %get-tuple-element.406, pred[1024,1024]{0,1:T(8,128)(4,1)S(1)} %broadcast_compare_fusion), kind=kLoop, calls=%fused_computation.5 | loop fusion | flops 12578816 | bytes 17858560 | tf_op jit(solution)/shard_map/while/body/eval_jaxpr/cond/branch_1_fun/reduce_sum | solution.py:33
  165.9 1.3 divide_convert_fusion
  167.3 0.4 all_to_all.20
  167.6 0.9 copy.43
  168.5 3.7 all-to-all-start
  172.2 8.6 %all-to-all-done = bf16[4,256,256]{1,2,0:T(8,128)(2,1)S(1)} async-done(((bf16[4,256,256]{1,2,0:T(8,128)(2,1)}), bf16[4,256,256]{1,2,0:T(8,128)(2,1)S(1)}, u32[]{:S(2)}, u32[]{:S(2)}) %all-to-all-start) | async-done | bytes 524320 | tf_op jit(solution)/shard_map/all_to_all | solution.py:102
  180.8 3.6 multiply_reduce_fusion.2
  184.4 0.0 copy-done.2
  184.4 0.0 copy-done.4
  184.4 0.4 add_convert_fusion
  184.8 0.3 fusion.13
  185.1 0.0 copy-done.5
  185.1 0.3 fusion.15
  185.5 2.6 broadcast_in_dim.62
  188.0 4.1 reshape.167
  192.1 6.6 %scatter_custom_fusion = bf16[704,2048]{1,0:T(8,128)(2,1)} fusion(s32[512]{0:T(512)S(1)} %bitcast.65, bf16[512,2048]{1,0:T(8,128)(2,1)} %reshape.167, bf16[]{:T(256)} %constant.98.clone.1), kind=kCustom, calls=%fused_computation.38 | custom fusion | bytes 2884096 | tf_op jit(solution)/shard_map/scatter | solution.py:117
  198.7 4.4 reshape.150
  203.2 261.2 %all_to_all.29 = bf16[32,22,2048]{2,1,0:T(8,128)(2,1)} all-to-all(bf16[32,22,2048]{2,1,0:T(8,128)(2,1)} %reshape.150), channel_id=1, replica_groups=mesh['sp'=8,'tp'=4] {'sp','tp'}, dimensions={0} | all-to-all | bytes 5767168 | tf_op jit(solution)/shard_map/all_to_all | solution.py:120
  464.4 4.5 reshape.151
  468.8 5.2 fusion.20
  474.0 0.0 copy-done
  474.0 7.7 %convolution_convert_fusion = bf16[704,2048]{1,0:T(8,128)(2,1)} fusion(bf16[1,512,2048]{2,1,0:T(8,128)(2,1)S(1)} %copy-done, bf16[704,2048]{1,0:T(8,128)(2,1)} %reshape.151, bf16[1,2048,512]{2,1,0:T(8,128)(2,1)} %param.30, f32[704,512]{1,0:T(8,128)} %fusion.20), kind=kOutput, calls=%fused_computation.21 | convolution fusion | flops 2956394496 | bytes 11403264 | tf_op jit(solution)/shard_map/dot_general | solution.py:126
  481.8 4.5 reshape.152
  486.3 3.9 all-to-all-start.2
  490.1 0.0 copy-done.8
  490.1 0.1 copy.48
  490.3 71.5 %all-to-all-done.2 = bf16[32,22,2048]{2,1,0:T(8,128)(2,1)} async-done(((bf16[32,22,2048]{2,1,0:T(8,128)(2,1)}), bf16[32,22,2048]{2,1,0:T(8,128)(2,1)}, u32[]{:S(2)}, u32[]{:S(2)}) %all-to-all-start.2) | async-done | bytes 2883616 | tf_op jit(solution)/shard_map/all_to_all | solution.py:127
  561.8 4.5 reshape.153
  566.3 7.4 %gather_fusion = bf16[512,2048]{1,0:T(8,128)(2,1)} fusion(bf16[704,2048]{1,0:T(8,128)(2,1)} %reshape.153, s32[1024]{0:T(1024)S(1)} %pad_clamp_fusion), kind=kCustom, calls=%fused_computation | custom fusion | bytes 4196352 | tf_op jit(solution)/shard_map/gather | solution.py:134
  573.7 5.4 reshape.154
  579.1 8.9 %multiply_reduce_fusion = f32[256,2048]{1,0:T(8,128)S(1)} fusion(f32[256,2,2048]{2,1,0:T(2,128)} %reshape.154, f32[256,2]{1,0:T(8,128)S(1)} %copy.48), kind=kLoop, calls=%fused_computation.20 | loop fusion | flops 1572864 | bytes 6293504 | tf_op jit(solution)/shard_map/reduce_sum | solution.py:136
  588.0 0.2 multiply_reduce_fusion.1
  588.3 0.0 copy-done.6
  588.3 1.4 fusion.16
  (29 shorter events, 0.2 us)
Async XLA Ops:
  6.5 467.5 %copy-start = (bf16[1,512,2048]{2,1,0:T(8,128)(2,1)S(1)}, bf16[1,512,2048]{2,1,0:T(8,128)(2,1)}, u32[]{:S(2)}) copy-start(bf16[1,512,2048]{2,1,0:T(8,128)(2,1)} %param.31) | copy-start | bytes 6291460
  6.5 3.8 copy-start.7
  6.5 131.1 %all-gather.2.cloned.1.call-start = ((), (), s32[]{:S(2)}) async-start(), calls=%async_computation.3 | async-start | bytes 9437184 | tf_op jit(solution)/shard_map/all_gather | solution.py:83
  138.7 2.7 copy-start.3
  145.9 5.7 copy-start.1
  168.5 12.3 %all-to-all-start = ((bf16[4,256,256]{1,2,0:T(8,128)(2,1)}), bf16[4,256,256]{1,2,0:T(8,128)(2,1)S(1)}, u32[]{:S(2)}, u32[]{:S(2)}) async-start(bf16[4,256,256]{1,2,0:T(8,128)(2,1)} %copy.43), calls=%async_computation | async-start | bytes 1048576 | tf_op jit(solution)/shard_map/all_to_all | solution.py:102
  180.8 3.7 copy-start.2
  180.8 3.7 copy-start.4
  184.4 0.7 copy-start.5
  486.3 3.9 copy-start.8
  486.3 75.6 %all-to-all-start.2 = ((bf16[32,22,2048]{2,1,0:T(8,128)(2,1)}), bf16[32,22,2048]{2,1,0:T(8,128)(2,1)}, u32[]{:S(2)}, u32[]{:S(2)}) async-start(bf16[32,22,2048]{2,1,0:T(8,128)(2,1)} %reshape.152), calls=%async_computation.2 | async-start | bytes 6291456 | tf_op jit(solution)/shard_map/all_to_all | solution.py:127
  579.1 9.1 %copy-start.6 = (f32[2048]{0:T(1024)S(1)}, f32[2048]{0:T(1024)}, u32[]{:S(2)}) copy-start(f32[2048]{0:T(1024)} %param.26) | copy-start | bytes 24580
Sparse Core Ops, SparseCore 0:
  10.4 127.1 all-gather.1
where the time goes:
time: 599 us; the launch traced here: 597 us
  blocking collectives  261 us (44%)
  waiting for transfers between devices  202 us (34%)
  local copies, waits for them, and re-layouts  60.6 us (10%)
  matrix products  26.2 us (4%)
  other arithmetic  24.6 us (4%)
  between operations  13.6 us (2%)
  starting transfers between devices  7.53 us (1%)
    all_to_all x1, blocking collectives, local(): lax.all_to_all(outgoing, ('sp', 'tp'), split_axis=0, concat_axis=0, tiled...  261 us
    all_gather x1, waiting for transfers between devices, local(): piece = lax.all_gather(paired, 'sp', axis=1, tiled=True)  122 us
    all_to_all x1, waiting for transfers between devices, local(): lax.all_to_all(expert_out.reshape(sources, slots, width_here), ('sp', 'tp...  71.5 us
  transfers between devices with their start and end apart: 3, of which 3 were waited for; matrix products, arithmetic and copies ran while one was open for 1% of the time, Pallas kernels for 0%

commit v1 on v0

v1 whole, which is shorter than its diff:
```python
import functools
import math

import jax
import jax.numpy as jnp
from jax import lax
from jax.experimental import pallas as pl
from jax.experimental.pallas import tpu as pltpu
from jax.sharding import PartitionSpec as P

HEAD_DIM = 64
NORM_EPS = 1e-06
MASKED = -1e30


def rms_scale(rows, gain):
    mean_sq = jnp.mean(rows * rows, axis=-1, keepdims=True)
    return rows * lax.rsqrt(mean_sq + NORM_EPS) * gain


def bf16_parts(values):
    parts = []
    for _ in range(3):
        part = lax.reduce_precision(values, 8, 7)
        parts.append(part.astype(jnp.bfloat16))
        values = values - part
    return parts


def flash_kernel(q_ref, k_ref, v_ref, o_ref, *, block_q, block_k, tiles, rows_dev, sub, shares):
    tile = pl.program_id(0)
    rank = lax.rem(lax.axis_index("sp"), shares)
    queries = q_ref[...]

    def step(first, state, masked):
        peak, acc = state
        scores = lax.dot_general(
            queries,
            k_ref[pl.ds(first, block_k), :],
            (((1,), (1,)), ((), ())),
            preferred_element_type=jnp.float32,
        )
        if masked:
            row = lax.broadcasted_iota(jnp.int32, (block_q, 1), 0)
            pos = row // sub * rows_dev + rank * sub + row % sub
            key = lax.broadcasted_iota(jnp.int32, (1, block_k), 1)
            scores = jnp.where(key <= pos, scores, MASKED)
        new_peak = jnp.maximum(peak, jnp.max(scores, axis=1, keepdims=True))
        probs = jnp.exp(scores - new_peak).astype(jnp.bfloat16)
        acc = acc * jnp.exp(peak - new_peak) + jnp.dot(
            probs, v_ref[pl.ds(first, block_k), :], preferred_element_type=jnp.float32
        )
        return new_peak, acc

    state = (
        jnp.full((block_q, 1), MASKED, jnp.float32),
        jnp.zeros((block_q, v_ref.shape[1]), jnp.float32),
    )
    state = lax.fori_loop(
        0,
        tile,
        lambda i, state: step(pl.multiple_of(i * block_k, block_k), state, False),
        state,
    )
    _, acc = step(pl.multiple_of(tile * block_k, block_k), state, True)
    o_ref[...] = (acc[:, :HEAD_DIM] / acc[:, HEAD_DIM : HEAD_DIM + 1]).astype(o_ref.dtype)


def flash(q_aug, k_aug, v_aug, rows_dev, sub, shares, block_q):
    rows = q_aug.shape[0]
    tiles = rows // block_q
    body = functools.partial(
        flash_kernel,
        block_q=block_q,
        block_k=block_q * shares,
        tiles=tiles,
        rows_dev=rows_dev,
        sub=sub,
        shares=shares,
    )
    whole = pl.BlockSpec(memory_space=pltpu.VMEM)
    return pl.pallas_call(
        body,
        grid=(tiles,),
        out_shape=jax.ShapeDtypeStruct((rows, HEAD_DIM), jnp.bfloat16),
        in_specs=[pl.BlockSpec((block_q, q_aug.shape[1]), lambda i: (i, 0)), whole, whole],
        out_specs=pl.BlockSpec((block_q, HEAD_DIM), lambda i: (i, 0)),
        compiler_params=pltpu.CompilerParams(vmem_limit_bytes=50 * 2**20),
        name="flash",
    )(q_aug, k_aug, v_aug)


def local(
    queries,
    key_rows,
    value_rows,
    cum_gate,
    residual,
    out_weight,
    gain_mix,
    gain_pre,
    gain_post,
    route_ids,
    route_weight,
    w_gate,
    w_up,
    w_down,
):
    tok_dev, feature_width = queries.shape
    local_heads = feature_width // HEAD_DIM
    n_sp, n_tp = lax.axis_size("sp"), lax.axis_size("tp")
    shares = n_sp // local_heads
    rows_dev = residual.shape[0]
    sub = rows_dev // shares
    chunk = n_tp * sub
    half = chunk // 2
    q_send = queries.reshape(n_tp, shares, sub, local_heads, HEAD_DIM).transpose(3, 1, 0, 2, 4)
    q_send = q_send.reshape(n_sp, chunk, HEAD_DIM)
    q_send = jnp.concatenate((q_send[:, :half], q_send[:, half:]), axis=2)
    kv_send = jnp.concatenate(
        (
            key_rows.reshape(tok_dev, local_heads, HEAD_DIM),
            value_rows.reshape(tok_dev, local_heads, HEAD_DIM),
        ),
        axis=2,
    ).transpose(1, 0, 2)
    kv_send = jnp.repeat(kv_send, shares, axis=0)
    sent = jnp.concatenate((kv_send, q_send), axis=1)
    got = lax.all_to_all(sent, "sp", split_axis=0, concat_axis=0, tiled=True)
    kv = got[:, :tok_dev].reshape(n_sp * tok_dev, 2 * HEAD_DIM)
    q_got = got[:, tok_dev:]
    q_got = jnp.concatenate((q_got[..., :HEAD_DIM], q_got[..., HEAD_DIM:]), axis=1)
    q_got = q_got.reshape(n_sp * chunk, HEAD_DIM) * jnp.bfloat16(HEAD_DIM**-0.5)

    me = lax.axis_index("sp")
    gate = lax.dynamic_index_in_dim(cum_gate, me // shares, 0, keepdims=False)
    gate_q = gate.reshape(n_sp * n_tp, shares, sub)
    gate_q = lax.dynamic_index_in_dim(gate_q, me % shares, 1, keepdims=False).reshape(-1)
    ones_q = jnp.ones((n_sp * chunk,), jnp.bfloat16)
    ones_k = jnp.ones((n_sp * tok_dev,), jnp.bfloat16)
    side_q = jnp.stack(bf16_parts(gate_q) + [ones_q] * 3, axis=1)
    side_k = jnp.stack([ones_k] * 3 + bf16_parts(-gate), axis=1)
    pad = ((0, 0), (0, HEAD_DIM - 6))
    q_aug = jnp.concatenate((q_got, jnp.pad(side_q, pad)), axis=1)
    k_aug = jnp.concatenate((kv[:, :HEAD_DIM], jnp.pad(side_k, pad)), axis=1)
    lane = lax.broadcasted_iota(jnp.int32, (n_sp * tok_dev, HEAD_DIM), 1)
    v_aug = jnp.concatenate((kv[:, HEAD_DIM:], (lane == 0).astype(jnp.bfloat16)), axis=1)
    out = flash(q_aug, k_aug, v_aug, rows_dev, sub, shares, chunk)

    out = out.reshape(n_sp * n_tp, sub, HEAD_DIM)
    out = jnp.concatenate((out[:, : sub // 2], out[:, sub // 2 :]), axis=2)
    heads = lax.all_to_all(out, ("sp", "tp"), split_axis=0, concat_axis=0, tiled=True)
    heads = heads.reshape(local_heads, shares, n_tp, sub // 2, 2, HEAD_DIM)
    head_rows = heads.transpose(1, 4, 3, 2, 0, 5).reshape(rows_dev, n_tp * feature_width)
    projected = jnp.dot(head_rows, out_weight, preferred_element_type=jnp.float32)
    stream = (residual.astype(jnp.float32) + rms_scale(projected, gain_mix)).astype(jnp.bfloat16)
    stream_wide = lax.optimization_barrier(stream).astype(jnp.float32)
    normed = rms_scale(stream_wide, gain_pre).astype(jnp.bfloat16)
    top_count = route_ids.shape[1]
    experts_all = n_sp * n_tp
    capacity = max(2, (4 * rows_dev * top_count + 3 * experts_all - 1) // (3 * experts_all))
    capacity = (capacity + 7) // 8 * 8
    flat_ids = route_ids.reshape(-1)
    item = lax.iota(jnp.int32, rows_dev * top_count)
    earlier = (item[None, :] < item[:, None]) & (flat_ids[None, :] == flat_ids[:, None])
    slot_index = flat_ids * capacity + jnp.sum(earlier.astype(jnp.int32), axis=1)
    slot_index = slot_index.reshape(rows_dev, top_count)
    slots_all = experts_all * capacity
    slot = lax.iota(jnp.int32, slots_all)
    place = sum((slot_index[:, k, None] == slot).astype(jnp.bfloat16) for k in range(top_count))
    outgoing = lax.dot_general(
        place, normed, (((0,), (0,)), ((), ())), preferred_element_type=jnp.float32
    ).astype(jnp.bfloat16)
    outgoing = outgoing.reshape(experts_all, capacity, -1)
    arrived = lax.all_to_all(outgoing, ("sp", "tp"), split_axis=0, concat_axis=0, tiled=True)
    flat_rows = arrived.reshape(slots_all, -1)
    gate_act = jnp.dot(flat_rows, w_gate[0], preferred_element_type=jnp.float32)
    up_act = jnp.dot(flat_rows, w_up[0], preferred_element_type=jnp.float32)
    hidden = (jax.nn.silu(gate_act) * up_act).astype(jnp.bfloat16)
    expert_out = jnp.dot(hidden, w_down[0], preferred_element_type=jnp.float32).astype(jnp.bfloat16)
    returned = lax.all_to_all(
        expert_out.reshape(experts_all, capacity, -1),
        ("sp", "tp"),
        split_axis=0,
        concat_axis=0,
        tiled=True,
    ).reshape(slots_all, -1)
    weigh = sum(
        jnp.where(slot_index[:, k, None] == slot, route_weight[:, k, None], 0.0)
        for k in range(top_count)
    )
    combined = sum(
        jnp.dot(part, returned, preferred_element_type=jnp.float32) for part in bf16_parts(weigh)
    )
    return (stream_wide + rms_scale(combined, gain_post)).astype(jnp.bfloat16)


def solution(mesh):
    return jax.shard_map(
        local,
        mesh=mesh,
        in_specs=(
            P("sp", "tp"),
            P("sp", "tp"),
            P("sp", "tp"),
            P("tp", None),
            P(("sp", "tp"), None),
            P(),
            P(),
            P(),
            P(),
            P(("sp", "tp"), None),
            P(("sp", "tp"), None),
            P(("sp", "tp"), None, None),
            P(("sp", "tp"), None, None),
            P(("sp", "tp"), None, None),
        ),
        out_specs=P(("sp", "tp"), None),
        check_vma=False,
    )
```

time: 599 us -> 329 us (0.55)
  blocking collectives: 261 us -> 73.9 us
  waiting for transfers between devices: 202 us -> 142 us
  local copies, waits for them, and re-layouts: 60.6 us -> 24 us
  Pallas kernels: 0 us -> 36.1 us
  other arithmetic: 24.6 us -> 11.4 us
  between operations: 13.6 us -> 0.4 us
  starting transfers between devices: 7.53 us -> 15.3 us
    all_to_all x1, blocking collectives: 261 us -> 73.9 us  [local(): lax.all_to_all(outgoing, ('sp', 'tp'), split_axis=0, concat_axis=0, tiled...]
    all_gather x1 -> x0, waiting for transfers between devices: 122 us -> none  [local(): piece = lax.all_gather(paired, 'sp', axis=1, tiled=True)]
    all_to_all x2 -> x3, waiting for transfers between devices: 80.1 us -> 142 us  [the longest x1 71.4 us: local(): lax.all_to_all(expert_out.reshape(experts_all, capacity, -1), ('sp', 'tp'...]
    pallas_call x0 -> x1, Pallas kernels: none -> 36.1 us  [flash(): pl.pallas_call(body, grid=(tiles,), out_shape=jax.ShapeDtypeStruct((rows,...]
    reduce_sum x3 -> x1, other arithmetic: 17.8 us -> 0.26 us  [local(): jnp.sum(earlier.astype(jnp.int32), axis=1)]
    reshape x5 -> x4, local copies, waits for them, and re-layouts: 22 us -> 5.39 us  [the longest x1 2.44 us: local(): heads = heads.reshape(local_heads, shares, n_tp, sub // 2, 2, HEAD_DIM)]
    all_to_all x2 -> x3, starting transfers between devices: 7.52 us -> 15.3 us  [the longest x1 7.28 us: local(): got = lax.all_to_all(sent, 'sp', split_axis=0, concat_axis=0, tiled=True)]
    gather x1 -> x0, local copies, waits for them, and re-layouts: 7.4 us -> none  [local(): picked = returned.reshape(experts_all * capacity, model_width)[slot_index]]
where the time goes in v1:
time: 329 us; the launch traced here: 328 us
  waiting for transfers between devices  142 us (43%)
  blocking collectives  73.9 us (22%)
  Pallas kernels  36.1 us (11%)
  matrix products  25.3 us (8%)
  local copies, waits for them, and re-layouts  24 us (7%)
  starting transfers between devices  15.3 us (5%)
  other arithmetic  11.4 us (3%)
    all_to_all x1, blocking collectives, local(): lax.all_to_all(outgoing, ('sp', 'tp'), split_axis=0, concat_axis=0, tiled...  73.9 us
    all_to_all x1, waiting for transfers between devices, local(): lax.all_to_all(expert_out.reshape(experts_all, capacity, -1), ('sp', 'tp'...  71.4 us
    all_to_all x1, waiting for transfers between devices, local(): got = lax.all_to_all(sent, 'sp', split_axis=0, concat_axis=0, tiled=True)  55.6 us
    pallas_call x1, Pallas kernels, flash(): pl.pallas_call(body, grid=(tiles,), out_shape=jax.ShapeDtypeStruct((rows,...  36.1 us
    all_to_all x1, waiting for transfers between devices, local(): lax.all_to_all(out, ('sp', 'tp'), split_axis=0, concat_axis=0, tiled=True)  14.6 us
    dot_general x3, matrix products, local(): jnp.dot(part, returned, preferred_element_type=jnp.float32)  9.39 us
    dot_general x1, matrix products, local(): jnp.dot(hidden, w_down[0], preferred_element_type=jnp.float32)  8.12 us
    all_to_all x1, starting transfers between devices, local(): got = lax.all_to_all(sent, 'sp', split_axis=0, concat_axis=0, tiled=True)  7.28 us
  transfers between devices with their start and end apart: 3, of which 3 were waited for; matrix products, arithmetic and copies ran while one was open for 1% of the time, Pallas kernels for 0%

profile of v1, /device:TPU:0, one launch (start us, length us, event | category | flops | bytes accessed | tf_op | source)
XLA Modules:
  0.0 328.0 jit_solution(13360507484839951583)
XLA Ops:
  0.0 1.4 copy.69
  1.4 0.4 reshape.176
  1.8 0.1 copy.70
  1.9 0.2 reshape.177
  2.1 0.0 copy-start.5
  2.1 0.1 fusion.58
  2.2 1.0 copy.71
  3.3 0.2 copy.67
  3.5 1.2 copy.66
  4.7 1.0 maximum_bitcast_fusion
  5.8 1.6 copy.68
  7.4 0.3 broadcast_in_dim.37
  7.7 0.8 copy-done.3
  8.4 1.7 pad_maximum_fusion
  10.1 7.3 %all-to-all-start = ((bf16[8,1280,128]{2,1,0:T(8,128)(2,1)}), bf16[8,1280,128]{2,1,0:T(8,128)(2,1)}, u32[]{:S(2)}, u32[]{:S(2)}) async-start(bf16[8,1280,128]{2,1,0:T(8,128)(2,1)} %pad_maximum_fusion), calls=%async_computation | async-start | bytes 5242880 | tf_op jit(solution)/shard_map/all_to_all | solution.py:129
  17.4 1.0 fusion.48
  18.4 0.1 fusion.50
  18.5 0.1 stack.9
  18.6 0.5 copy.72
  19.2 0.2 stack.21
  19.5 1.9 copy.73
  21.3 0.1 pad.13.clone
  21.4 55.6 %all-to-all-done = bf16[8,1280,128]{2,1,0:T(8,128)(2,1)} async-done(((bf16[8,1280,128]{2,1,0:T(8,128)(2,1)}), bf16[8,1280,128]{2,1,0:T(8,128)(2,1)}, u32[]{:S(2)}, u32[]{:S(2)}) %all-to-all-start) | async-done | bytes 2621472 | tf_op jit(solution)/shard_map/all_to_all | solution.py:129
  77.0 1.7 slice.61
  78.7 0.7 fusion.56
  79.5 1.5 fusion.55
  81.0 0.3 maximum_multiply_fusion
  81.3 0.6 fusion.14.q_ref
  81.9 0.9 copy-done.1
  82.8 3.2 fusion.5
  86.1 36.1 %flash.1 = bf16[4096,64]{1,0:T(8,128)(2,1)S(1)} custom-call(bf16[4096,128]{1,0:T(8,128)(2,1)S(1)} %fusion.14.q_ref, bf16[8192,128]{1,0:T(8,128)(2,1)} %get-tuple-element.28.k_ref, bf16[8192,128]{1,0:T(8,128)(2,1)} %get-tuple-element.29.v_ref), custom_call_target="tpu_custom_call" | custom-call | tf_op jit(solution)/shard_map/flash/pallas_call | solution.py:82
  122.2 0.0 copy-start.8
  122.2 0.1 fusion.57
  122.3 1.1 pad_maximum_fusion.3
  123.4 4.0 %all-to-all-start.1 = ((bf16[32,64,128]{2,1,0:T(8,128)(2,1)}), bf16[32,64,128]{2,1,0:T(8,128)(2,1)}, u32[]{:S(2)}, u32[]{:S(2)}) async-start(bf16[32,64,128]{2,1,0:T(8,128)(2,1)} %pad_maximum_fusion.3), calls=%async_computation.1 | async-start | bytes 1048576 | tf_op jit(solution)/shard_map/all_to_all | solution.py:152
  127.4 0.1 copy.75
  127.6 0.1 eq.33
  127.7 0.3 convert_reduce_fusion
  128.0 0.1 reduce_sum.40
  128.1 0.1 copy.76
  128.2 14.6 %all-to-all-done.1 = bf16[32,64,128]{2,1,0:T(8,128)(2,1)} async-done(((bf16[32,64,128]{2,1,0:T(8,128)(2,1)}), bf16[32,64,128]{2,1,0:T(8,128)(2,1)}, u32[]{:S(2)}, u32[]{:S(2)}) %all-to-all-start.1) | async-done | bytes 524320 | tf_op jit(solution)/shard_map/all_to_all | solution.py:152
  142.8 2.4 reshape.182
  145.3 1.8 copy.74
  147.1 2.4 reshape.183
  149.4 0.0 copy-start.4
  149.5 0.0 copy-start.6
  149.5 3.6 %multiply_reduce_fusion.1 = (f32[256]{0:T(256)S(1)}, f32[256,2048]{1,0:T(8,128)S(1)}) fusion(bf16[256,1024]{1,0:T(8,128)(2,1)S(1)} %reshape.183, bf16[1024,2048]{1,0:T(8,128)(2,1)} %param.19), kind=kOutput, calls=%fused_computation.24 | convolution fusion | flops 1074790144 | bytes 6816768 | tf_op jit(solution)/shard_map/dot_general | solution.py:155
  153.1 0.0 copy-start.11
  153.1 0.4 add_convert_fusion
  153.5 0.3 fusion.1
  153.8 0.0 copy-done.11
  153.8 1.2 convolution_convert_fusion.1
  155.1 0.0 copy-start.10
  155.1 73.9 %all_to_all.20 = bf16[32,24,2048]{2,1,0:T(8,128)(2,1)S(1)} all-to-all(bf16[32,24,2048]{2,1,0:T(8,128)(2,1)S(1)} %bitcast.65), channel_id=1, replica_groups=mesh['sp'=8,'tp'=4] {'sp','tp'}, dimensions={0} | all-to-all | bytes 6291456 | tf_op jit(solution)/shard_map/all_to_all | solution.py:175
  229.0 1.7 copy-done.2
  230.7 3.0 fusion.9
  233.6 8.1 %convolution_convert_fusion = bf16[768,2048]{1,0:T(8,128)(2,1)} fusion(bf16[1,512,2048]{2,1,0:T(8,128)(2,1)S(1)} %copy-done, f32[768,512]{1,0:T(8,128)} %fusion.9, bf16[768,2048]{1,0:T(8,128)(2,1)} %bitcast.64, bf16[1,2048,512]{2,1,0:T(8,128)(2,1)} %param.26), kind=kOutput, calls=%fused_computation.2 | convolution fusion | flops 3225157632 | bytes 12058624 | tf_op jit(solution)/shard_map/dot_general | solution.py:180
  241.8 4.0 %all-to-all-start.3 = ((bf16[32,24,2048]{2,1,0:T(8,128)(2,1)}), bf16[32,24,2048]{2,1,0:T(8,128)(2,1)}, u32[]{:S(2)}, u32[]{:S(2)}) async-start(bf16[32,24,2048]{2,1,0:T(8,128)(2,1)} %bitcast.62), calls=%async_computation.3 | async-start | bytes 6291456 | tf_op jit(solution)/shard_map/all_to_all | solution.py:181
  245.8 71.4 %all-to-all-done.3 = bf16[32,24,2048]{2,1,0:T(8,128)(2,1)} async-done(((bf16[32,24,2048]{2,1,0:T(8,128)(2,1)}), bf16[32,24,2048]{2,1,0:T(8,128)(2,1)}, u32[]{:S(2)}, u32[]{:S(2)}) %all-to-all-start.3) | async-done | bytes 3145760 | tf_op jit(solution)/shard_map/all_to_all | solution.py:181
  317.1 3.0 fusion.26
  320.2 3.1 convolution_add_fusion.1
  323.3 0.0 copy-start.7
  323.3 3.2 multiply_reduce_fusion
  326.6 1.4 fusion.4
  (26 shorter events, 0.2 us)
Async XLA Ops:
  0.0 233.6 %copy-start = (bf16[1,512,2048]{2,1,0:T(8,128)(2,1)S(1)}, bf16[1,512,2048]{2,1,0:T(8,128)(2,1)}, u32[]{:S(2)}) copy-start(bf16[1,512,2048]{2,1,0:T(8,128)(2,1)} %param.27) | copy-start | bytes 6291460
  2.1 1.1 copy-start.5
  7.4 1.0 copy-start.3
  10.1 66.9 %all-to-all-start = ((bf16[8,1280,128]{2,1,0:T(8,128)(2,1)}), bf16[8,1280,128]{2,1,0:T(8,128)(2,1)}, u32[]{:S(2)}, u32[]{:S(2)}) async-start(bf16[8,1280,128]{2,1,0:T(8,128)(2,1)} %pad_maximum_fusion), calls=%async_computation | async-start | bytes 5242880 | tf_op jit(solution)/shard_map/all_to_all | solution.py:129
  81.3 1.6 copy-start.1
  122.2 5.2 %copy-start.8 = (s32[256,2]{0,1:T(2,128)S(1)}, s32[256,2]{0,1:T(2,128)}, u32[]{:S(2)}) copy-start(s32[256,2]{0,1:T(2,128)} %param.23) | copy-start | bytes 6148
  123.4 19.4 %all-to-all-start.1 = ((bf16[32,64,128]{2,1,0:T(8,128)(2,1)}), bf16[32,64,128]{2,1,0:T(8,128)(2,1)}, u32[]{:S(2)}, u32[]{:S(2)}) async-start(bf16[32,64,128]{2,1,0:T(8,128)(2,1)} %pad_maximum_fusion.3), calls=%async_computation.1 | async-start | bytes 1048576 | tf_op jit(solution)/shard_map/all_to_all | solution.py:152
  149.4 3.7 %copy-start.4 = (bf16[256,2048]{1,0:T(8,128)(2,1)S(1)}, bf16[256,2048]{1,0:T(8,128)(2,1)}, u32[]{:S(2)}) copy-start(bf16[256,2048]{1,0:T(8,128)(2,1)} %param.18) | copy-start | bytes 3145732
  149.5 3.6 %copy-start.6 = (f32[2048]{0:T(1024)S(1)}, f32[2048]{0:T(1024)}, u32[]{:S(2)}) copy-start(f32[2048]{0:T(1024)} %param.20) | copy-start | bytes 24580
  153.1 0.7 copy-start.11
  155.1 75.6 %copy-start.10 = (bf16[1,2048,512]{2,1,0:T(8,128)(2,1)S(1)}, bf16[1,2048,512]{2,1,0:T(8,128)(2,1)}, u32[]{:S(2)}) copy-start(bf16[1,2048,512]{2,1,0:T(8,128)(2,1)} %param.25) | copy-start | bytes 6291460
  229.0 1.7 copy-start.2
  241.8 4.0 %copy-start.9 = (f32[256,2]{0,1:T(2,128)S(1)}, f32[256,2]{0,1:T(2,128)}, u32[]{:S(2)}) copy-start(f32[256,2]{0,1:T(2,128)} %param.24) | copy-start | bytes 6148
  241.8 75.4 %all-to-all-start.3 = ((bf16[32,24,2048]{2,1,0:T(8,128)(2,1)}), bf16[32,24,2048]{2,1,0:T(8,128)(2,1)}, u32[]{:S(2)}, u32[]{:S(2)}) async-start(bf16[32,24,2048]{2,1,0:T(8,128)(2,1)} %bitcast.62), calls=%async_computation.3 | async-start | bytes 6291456 | tf_op jit(solution)/shard_map/all_to_all | solution.py:181
  323.3 3.3 copy-start.7

commit v2 on v1

--- a/solution.py
+++ b/solution.py
@@ -27,67 +27,175 @@
     return parts
 
 
-def flash_kernel(q_ref, k_ref, v_ref, o_ref, *, block_q, block_k, tiles, rows_dev, sub, shares):
+def pack_kernel(q_ref, k_ref, v_ref, one_ref, two_ref, *, shares, n_tp):
+    tok_dev, width = q_ref.shape
+    first = tok_dev - two_ref.shape[1]
+    rows_dev = tok_dev // n_tp
+    sub = rows_dev // shares
+    for h in range(width // HEAD_DIM):
+        cols = pl.ds(h * HEAD_DIM, HEAD_DIM)
+        pairs = jnp.concatenate((k_ref[:, cols], v_ref[:, cols]), axis=1)
+        for r in range(shares):
+            dest = h * shares + r
+            one_ref[dest, :first] = pairs[:first]
+            two_ref[dest] = pairs[first:]
+            for t in range(n_tp // 2):
+                low, high = (
+                    q_ref[pl.ds((t + step) * rows_dev + r * sub, sub), cols]
+                    for step in (0, n_tp // 2)
+                )
+                one_ref[dest, pl.ds(first + t * sub, sub)] = jnp.concatenate((low, high), axis=1)
+
+
+def pack(queries, key_rows, value_rows, first, shares, n_tp):
+    tok_dev, width = queries.shape
+    dests = width // HEAD_DIM * shares
+    half = tok_dev // shares // 2
+    shapes = [(dests, first + half, 2 * HEAD_DIM), (dests, tok_dev - first, 2 * HEAD_DIM)]
+    return pl.pallas_call(
+        functools.partial(pack_kernel, shares=shares, n_tp=n_tp),
+        out_shape=[jax.ShapeDtypeStruct(shape, jnp.bfloat16) for shape in shapes],
+        in_specs=[pl.BlockSpec(memory_space=pltpu.VMEM)] * 3,
+        out_specs=[pl.BlockSpec(memory_space=pltpu.VMEM)] * 2,
+        compiler_params=pltpu.CompilerParams(vmem_limit_bytes=32 * 2**20),
+        name="pack",
+    )(queries, key_rows, value_rows)
+
+
+def assemble_kernel(in_ref, out_ref, *, shares, n_tp, local_heads):
+    half = in_ref.shape[1]
+    for t in range(n_tp):
+        for h in range(0, local_heads, 2):
+            for r in range(shares):
+                left = in_ref[(h * shares + r) * n_tp + t]
+                right = in_ref[((h + 1) * shares + r) * n_tp + t]
+                for part in range(2):
+                    cols = slice(part * HEAD_DIM, (part + 1) * HEAD_DIM)
+                    out_ref[
+                        pl.ds((2 * r + part) * half, half),
+                        pl.ds((t * local_heads + h) * HEAD_DIM, 2 * HEAD_DIM),
+                    ] = jnp.concatenate((left[:, cols], right[:, cols]), axis=1)
+
+
+def assemble(heads, shares, n_tp, local_heads):
+    shape = (2 * shares * heads.shape[1], n_tp * local_heads * HEAD_DIM)
+    return pl.pallas_call(
+        functools.partial(
+            assemble_kernel, shares=shares, n_tp=n_tp, local_heads=local_heads
+        ),
+        out_shape=jax.ShapeDtypeStruct(shape, jnp.bfloat16),
+        in_specs=[pl.BlockSpec(memory_space=pltpu.VMEM)],
+        out_specs=pl.BlockSpec(memory_space=pltpu.VMEM),
+        name="assemble",
+    )(heads)
+
+
+def flash_kernel(*refs, begun, span, shares, sub, rows_dev, n_tp):
+    if begun:
+        q_ref, kv_ref, side_q_ref, side_k_ref, state_ref, o_ref, k_aug, v_aug = refs
+    else:
+        q_ref, kv_ref, side_q_ref, side_k_ref, o_ref, k_aug, v_aug = refs
+    lo, hi = span
+    count = hi - lo
     tile = pl.program_id(0)
     rank = lax.rem(lax.axis_index("sp"), shares)
-    queries = q_ref[...]
-
-    def step(first, state, masked):
+
+    @pl.when(tile == 0)
+    def _():
+        lane = lax.broadcasted_iota(jnp.int32, (count, 2 * HEAD_DIM), 1)
+
+        def one(src, carry):
+            kv = kv_ref[src, :count].astype(jnp.float32)
+            side = side_k_ref[src, lo:hi].astype(jnp.float32)
+            k_aug[src] = jnp.where(lane < HEAD_DIM, kv, side).astype(jnp.bfloat16)
+            ones = (lane == 0).astype(jnp.float32)
+            v_aug[src] = jnp.where(lane < HEAD_DIM, ones, kv).astype(jnp.bfloat16)
+            return carry
+
+        lax.fori_loop(0, kv_ref.shape[0], one, 0)
+
+    packed = q_ref[0]
+    queries = jnp.concatenate((packed[:, :HEAD_DIM], packed[:, HEAD_DIM:]), axis=0)
+    queries = queries * jnp.bfloat16(HEAD_DIM**-0.5)
+    queries = jnp.concatenate((queries, side_q_ref[:, HEAD_DIM:]), axis=1)
+    rows = queries.shape[0]
+    out_lane = lax.broadcasted_iota(jnp.int32, (rows, 2 * HEAD_DIM), 1)
+
+    def step(src, state, masked):
         peak, acc = state
         scores = lax.dot_general(
-            queries,
-            k_ref[pl.ds(first, block_k), :],
-            (((1,), (1,)), ((), ())),
-            preferred_element_type=jnp.float32,
+            queries, k_aug[src], (((1,), (1,)), ((), ())), preferred_element_type=jnp.float32
         )
         if masked:
-            row = lax.broadcasted_iota(jnp.int32, (block_q, 1), 0)
+            row = lax.broadcasted_iota(jnp.int32, (rows, 1), 0)
             pos = row // sub * rows_dev + rank * sub + row % sub
-            key = lax.broadcasted_iota(jnp.int32, (1, block_k), 1)
+            key = lo + lax.broadcasted_iota(jnp.int32, (1, count), 1)
             scores = jnp.where(key <= pos, scores, MASKED)
         new_peak = jnp.maximum(peak, jnp.max(scores, axis=1, keepdims=True))
         probs = jnp.exp(scores - new_peak).astype(jnp.bfloat16)
         acc = acc * jnp.exp(peak - new_peak) + jnp.dot(
-            probs, v_ref[pl.ds(first, block_k), :], preferred_element_type=jnp.float32
+            probs, v_aug[src], preferred_element_type=jnp.float32
         )
         return new_peak, acc
 
-    state = (
-        jnp.full((block_q, 1), MASKED, jnp.float32),
-        jnp.zeros((block_q, v_ref.shape[1]), jnp.float32),
-    )
-    state = lax.fori_loop(
-        0,
-        tile,
-        lambda i, state: step(pl.multiple_of(i * block_k, block_k), state, False),
-        state,
-    )
-    _, acc = step(pl.multiple_of(tile * block_k, block_k), state, True)
-    o_ref[...] = (acc[:, :HEAD_DIM] / acc[:, HEAD_DIM : HEAD_DIM + 1]).astype(o_ref.dtype)
-
-
-def flash(q_aug, k_aug, v_aug, rows_dev, sub, shares, block_q):
-    rows = q_aug.shape[0]
-    tiles = rows // block_q
+    if begun:
+        before = state_ref[...]
+        state = (before[:, 1:2], jnp.where(out_lane == 1, 0.0, before))
+    else:
+        state = (
+            jnp.full((rows, 1), MASKED, jnp.float32),
+            jnp.zeros((rows, 2 * HEAD_DIM), jnp.float32),
+        )
+    state = lax.fori_loop(0, tile, lambda i, state: step(i, state, False), state)
+    peak, acc = step(tile, state, True)
+    if not begun:
+        o_ref[...] = jnp.where(out_lane == 1, peak, acc)
+        return
+    out = acc[:, HEAD_DIM:] / acc[:, :1]
+    half = sub // 2
+    for t in range(n_tp):
+        top, low = (out[t * sub + step : t * sub + step + half] for step in (0, half))
+        o_ref[t] = jnp.concatenate((top, low), axis=1).astype(o_ref.dtype)
+
+
+def flash(got, kv, side_q, side_k, state, span, first, sub, rows_dev, n_tp, shares):
+    n_sp, count = kv.shape[0], span[1] - span[0]
+    chunk = n_tp * sub
+    lanes = 2 * HEAD_DIM
+    whole = pl.BlockSpec(memory_space=pltpu.VMEM)
+    begun = state is not None
+    wide = pl.BlockSpec((chunk, lanes), lambda i: (i, 0))
+    if begun:
+        out_shape = jax.ShapeDtypeStruct((n_sp * n_tp, sub // 2, lanes), jnp.bfloat16)
+        out_spec = pl.BlockSpec((n_tp, sub // 2, lanes), lambda i: (i, 0, 0))
+    else:
+        out_shape = jax.ShapeDtypeStruct((n_sp * chunk, lanes), jnp.float32)
+        out_spec = wide
+    first_q = first // (chunk // 2)
     body = functools.partial(
         flash_kernel,
-        block_q=block_q,
-        block_k=block_q * shares,
-        tiles=tiles,
+        begun=begun,
+        span=span,
+        shares=shares,
+        sub=sub,
         rows_dev=rows_dev,
-        sub=sub,
-        shares=shares,
+        n_tp=n_tp,
     )
-    whole = pl.BlockSpec(memory_space=pltpu.VMEM)
+    q_spec = pl.BlockSpec((1, chunk // 2, lanes), lambda i: (i, first_q, 0))
+    pairs = n_sp * (n_sp + 1) // 2 * chunk * count
     return pl.pallas_call(
         body,
-        grid=(tiles,),
-        out_shape=jax.ShapeDtypeStruct((rows, HEAD_DIM), jnp.bfloat16),
-        in_specs=[pl.BlockSpec((block_q, q_aug.shape[1]), lambda i: (i, 0)), whole, whole],
-        out_specs=pl.BlockSpec((block_q, HEAD_DIM), lambda i: (i, 0)),
+        grid=(n_sp,),
+        out_shape=out_shape,
+        in_specs=[q_spec, whole, wide, whole] + [wide] * begun,
+        out_specs=out_spec,
+        scratch_shapes=[pltpu.VMEM((n_sp, count, lanes), jnp.bfloat16)] * 2,
         compiler_params=pltpu.CompilerParams(vmem_limit_bytes=50 * 2**20),
+        cost_estimate=pl.CostEstimate(
+            flops=8 * lanes * pairs, bytes_accessed=2**22, transcendentals=pairs
+        ),
         name="flash",
-    )(q_aug, k_aug, v_aug)
+    )(got, kv, side_q, side_k, *([state] if begun else []))
 
 
 def local(
@@ -114,23 +222,11 @@
     sub = rows_dev // shares
     chunk = n_tp * sub
     half = chunk // 2
-    q_send = queries.reshape(n_tp, shares, sub, local_heads, HEAD_DIM).transpose(3, 1, 0, 2, 4)
-    q_send = q_send.reshape(n_sp, chunk, HEAD_DIM)
-    q_send = jnp.concatenate((q_send[:, :half], q_send[:, half:]), axis=2)
-    kv_send = jnp.concatenate(
-        (
-            key_rows.reshape(tok_dev, local_heads, HEAD_DIM),
-            value_rows.reshape(tok_dev, local_heads, HEAD_DIM),
-        ),
-        axis=2,
-    ).transpose(1, 0, 2)
-    kv_send = jnp.repeat(kv_send, shares, axis=0)
-    sent = jnp.concatenate((kv_send, q_send), axis=1)
-    got = lax.all_to_all(sent, "sp", split_axis=0, concat_axis=0, tiled=True)
-    kv = got[:, :tok_dev].reshape(n_sp * tok_dev, 2 * HEAD_DIM)
-    q_got = got[:, tok_dev:]
-    q_got = jnp.concatenate((q_got[..., :HEAD_DIM], q_got[..., HEAD_DIM:]), axis=1)
-    q_got = q_got.reshape(n_sp * chunk, HEAD_DIM) * jnp.bfloat16(HEAD_DIM**-0.5)
+    first = tok_dev * 5 // 8 // half * half
+    one, two = pack(queries, key_rows, value_rows, first, shares, n_tp)
+    got = lax.all_to_all(one, "sp", split_axis=0, concat_axis=0, tiled=True)
+    got, two = lax.optimization_barrier((got, two))
+    got_two = lax.all_to_all(two, "sp", split_axis=0, concat_axis=0, tiled=True)
 
     me = lax.axis_index("sp")
     gate = lax.dynamic_index_in_dim(cum_gate, me // shares, 0, keepdims=False)
@@ -140,18 +236,14 @@
     ones_k = jnp.ones((n_sp * tok_dev,), jnp.bfloat16)
     side_q = jnp.stack(bf16_parts(gate_q) + [ones_q] * 3, axis=1)
     side_k = jnp.stack([ones_k] * 3 + bf16_parts(-gate), axis=1)
-    pad = ((0, 0), (0, HEAD_DIM - 6))
-    q_aug = jnp.concatenate((q_got, jnp.pad(side_q, pad)), axis=1)
-    k_aug = jnp.concatenate((kv[:, :HEAD_DIM], jnp.pad(side_k, pad)), axis=1)
-    lane = lax.broadcasted_iota(jnp.int32, (n_sp * tok_dev, HEAD_DIM), 1)
-    v_aug = jnp.concatenate((kv[:, HEAD_DIM:], (lane == 0).astype(jnp.bfloat16)), axis=1)
-    out = flash(q_aug, k_aug, v_aug, rows_dev, sub, shares, chunk)
-
-    out = out.reshape(n_sp * n_tp, sub, HEAD_DIM)
-    out = jnp.concatenate((out[:, : sub // 2], out[:, sub // 2 :]), axis=2)
+    pad = ((0, 0), (HEAD_DIM, HEAD_DIM - 6))
+    side_q = jnp.pad(side_q, pad)
+    side_k = jnp.pad(side_k, pad).reshape(n_sp, tok_dev, 2 * HEAD_DIM)
+    fixed = (first, sub, rows_dev, n_tp, shares)
+    state = flash(got, got, side_q, side_k, None, (0, first), *fixed)
+    out = flash(got, got_two, side_q, side_k, state, (first, tok_dev), *fixed)
     heads = lax.all_to_all(out, ("sp", "tp"), split_axis=0, concat_axis=0, tiled=True)
-    heads = heads.reshape(local_heads, shares, n_tp, sub // 2, 2, HEAD_DIM)
-    head_rows = heads.transpose(1, 4, 3, 2, 0, 5).reshape(rows_dev, n_tp * feature_width)
+    head_rows = assemble(heads, shares, n_tp, local_heads)
     projected = jnp.dot(head_rows, out_weight, preferred_element_type=jnp.float32)
     stream = (residual.astype(jnp.float32) + rms_scale(projected, gain_mix)).astype(jnp.bfloat16)
     stream_wide = lax.optimization_barrier(stream).astype(jnp.float32)

time: 329 us -> 332 us (level)
  Pallas kernels: 36.1 us -> 70 us
  waiting for transfers between devices: 142 us -> 121 us
  local copies, waits for them, and re-layouts: 24 us -> 15.9 us
  other arithmetic: 11.4 us -> 3.4 us
  starting transfers between devices: 15.3 us -> 21.3 us
    pallas_call x1 -> x4, Pallas kernels: 36.1 us -> 70 us  [the longest x2 66.6 us: flash(): pl.pallas_call(body, grid=(n_sp,), out_shape=out_shape, in_specs=[q_spec,...]
    all_to_all x1 -> x2, waiting for transfers between devices: 55.6 us -> 34.5 us  [the longest x1 34.5 us: local(): got = lax.all_to_all(one, 'sp', split_axis=0, concat_axis=0, tiled=True)]
    concatenate x5 -> x0, other arithmetic: 6.71 us -> none  [the longest x1 3.24 us: local(): k_aug = jnp.concatenate((kv[:, :HEAD_DIM], jnp.pad(side_k, pad)), axis=1)]
    reshape x4 -> x0, local copies, waits for them, and re-layouts: 5.39 us -> none  [the longest x1 2.44 us: local(): heads = heads.reshape(local_heads, shares, n_tp, sub // 2, 2, HEAD_DIM)]
    all_to_all x1 -> x2, starting transfers between devices: 7.28 us -> 11.5 us  [the longest x1 7.28 us: local(): got = lax.all_to_all(one, 'sp', split_axis=0, concat_axis=0, tiled=True)]
    slice x5 -> x0, local copies, waits for them, and re-layouts: 4.1 us -> none  [the longest x1 1.74 us: local(): kv = got[:, :tok_dev].reshape(n_sp * tok_dev, 2 * HEAD_DIM)]
    pad x0 -> x2, local copies, waits for them, and re-layouts: none -> 3.82 us  [the longest x1 2.06 us: local(): side_k = jnp.pad(side_k, pad).reshape(n_sp, tok_dev, 2 * HEAD_DIM)]
    transpose x3 -> x0, local copies, waits for them, and re-layouts: 3.53 us -> none  [the longest x1 1.78 us: local(): heads.transpose(1, 4, 3, 2, 0, 5).reshape(rows_dev, n_tp * feature_width)]
  transfers between devices with their start and end apart: 3 -> 4, of which waited for: 3 -> 3; matrix products, arithmetic and copies ran while one was open for 1% -> 3% of each run, Pallas kernels for 0% -> 8%
where the time goes in v2:
time: 332 us; the launch traced here: 331 us
  waiting for transfers between devices  121 us (36%)
  blocking collectives  73.9 us (22%)
  Pallas kernels  70 us (21%)
  matrix products  25.5 us (8%)
  starting transfers between devices  21.3 us (6%)
  local copies, waits for them, and re-layouts  15.9 us (5%)
  other arithmetic  3.4 us (1%)
    all_to_all x1, blocking collectives, local(): lax.all_to_all(outgoing, ('sp', 'tp'), split_axis=0, concat_axis=0, tiled...  73.9 us
    all_to_all x1, waiting for transfers between devices, local(): lax.all_to_all(expert_out.reshape(experts_all, capacity, -1), ('sp', 'tp'...  71.6 us
    pallas_call x2, Pallas kernels, flash(): pl.pallas_call(body, grid=(n_sp,), out_shape=out_shape, in_specs=[q_spec,...  66.6 us
    all_to_all x1, waiting for transfers between devices, local(): got = lax.all_to_all(one, 'sp', split_axis=0, concat_axis=0, tiled=True)  34.5 us
    all_to_all x1, waiting for transfers between devices, local(): lax.all_to_all(out, ('sp', 'tp'), split_axis=0, concat_axis=0, tiled=True)  14.8 us
    unnamed x34, local copies, waits for them, and re-layouts  9.89 us
    dot_general x3, matrix products, local(): jnp.dot(part, returned, preferred_element_type=jnp.float32)  9.39 us
    dot_general x1, matrix products, local(): jnp.dot(hidden, w_down[0], preferred_element_type=jnp.float32)  8.13 us
  transfers between devices with their start and end apart: 4, of which 3 were waited for; matrix products, arithmetic and copies ran while one was open for 3% of the time, Pallas kernels for 8%

profile of v2, /device:TPU:0, one launch (start us, length us, event | category | flops | bytes accessed | tf_op | source)
XLA Modules:
  0.0 331.2 jit_solution(6653220931960203042)
XLA Ops:
  0.0 0.0 copy-start
  0.0 0.0 copy-start.2
  0.0 1.2 copy-done.2
  1.2 0.0 copy-start.3
  1.2 1.0 copy-done.3
  2.2 0.0 copy-start.4
  2.2 1.0 copy-done.4
  3.3 1.4 pack.1
  4.7 0.0 copy-start.1
  4.7 1.2 copy-done.1
  5.9 7.3 %all-to-all-start = ((bf16[8,768,128]{2,1,0:T(8,128)(2,1)}), bf16[8,768,128]{2,1,0:T(8,128)(2,1)}, u32[]{:S(2)}, u32[]{:S(2)}) async-start(bf16[8,768,128]{2,1,0:T(8,128)(2,1)} %copy-done.1), calls=%async_computation | async-start | bytes 3145728 | tf_op jit(solution)/shard_map/all_to_all | solution.py:227
  13.1 1.0 fusion.44
  14.1 0.1 fusion.46
  14.2 0.1 stack.9
  14.3 1.4 copy.41
  15.8 34.5 %all-to-all-done.refs_0_.refs_1_ = bf16[8,768,128]{2,1,0:T(8,128)(2,1)} async-done(((bf16[8,768,128]{2,1,0:T(8,128)(2,1)}), bf16[8,768,128]{2,1,0:T(8,128)(2,1)}, u32[]{:S(2)}, u32[]{:S(2)}) %all-to-all-start) | async-done | bytes 1572896 | tf_op jit(solution)/shard_map/all_to_all | solution.py:227
  50.3 4.3 %all-to-all-start.1 = ((bf16[8,512,128]{2,1,0:T(8,128)(2,1)}), bf16[8,512,128]{2,1,0:T(8,128)(2,1)}, u32[]{:S(2)}, u32[]{:S(2)}) async-start(bf16[8,512,128]{2,1,0:T(8,128)(2,1)} %get-tuple-element.12), calls=%async_computation.1 | async-start | bytes 2097152 | tf_op jit(solution)/shard_map/all_to_all | solution.py:229
  54.6 0.2 stack.21
  54.9 1.9 copy.45
  56.7 1.8 pad.8.refs_2_
  58.5 0.1 copy-done.6
  58.7 2.1 pad.9.clone
  60.7 26.4 %flash.2.refs_4_ = f32[4096,128]{1,0:T(8,128)} custom-call(bf16[8,768,128]{2,1,0:T(8,128)(2,1)} %all-to-all-done.refs_0_.refs_1_, bf16[8,768,128]{2,1,0:T(8,128)(2,1)} %all-to-all-done.refs_0_.refs_1_, bf16[4096,128]{1,0:T(8,128)(2,1)S(1)} %pad.8.refs_2_, bf16[8,1024,128]{2,1,0:T(8,128)(2,1)} %bitcast.48), custom_call_target="tpu_custom_call" | custom-call | flops 9663676416 | bytes 4194304 | tf_op jit(solution)/shard_map/flash/pallas_call | solution.py:186
  87.2 0.0 copy-start.12
  87.2 0.0 all-to-all-done.1.refs_1_
  87.2 40.1 %flash.3 = bf16[32,64,128]{2,1,0:T(8,128)(2,1)S(1)} custom-call(bf16[8,768,128]{2,1,0:T(8,128)(2,1)} %all-to-all-done.refs_0_.refs_1_, bf16[8,512,128]{2,1,0:T(8,128)(2,1)} %all-to-all-done.1.refs_1_, bf16[4096,128]{1,0:T(8,128)(2,1)S(1)} %pad.8.refs_2_, bf16[8,1024,128]{2,1,0:T(8,128)(2,1)} %bitcast.49, f32[4096,128]{1,0:T(8,128)} %flash.2.refs_4_), custom_call_target="tpu_custom_call" | custom-call | flops 9663676416 | bytes 4194304 | tf_op jit(solution)/shard_map/flash/pallas_call | solution.py:186
  127.3 0.0 copy-start.5
  127.3 0.8 copy-done.5
  128.1 5.9 %all-to-all-start.2 = ((bf16[32,64,128]{2,1,0:T(8,128)(2,1)}), bf16[32,64,128]{2,1,0:T(8,128)(2,1)S(1)}, u32[]{:S(2)}, u32[]{:S(2)}) async-start(bf16[32,64,128]{2,1,0:T(8,128)(2,1)} %copy-done.5), calls=%async_computation.2 | async-start | bytes 1048576 | tf_op jit(solution)/shard_map/all_to_all | solution.py:245
  134.0 0.0 copy-done.12
  134.0 0.1 copy.43
  134.2 0.1 eq.26
  134.3 0.3 convert_reduce_fusion
  134.6 0.1 reduce_sum.40
  134.7 0.1 copy.44
  134.8 14.8 %all-to-all-done.2.in_ref = bf16[32,64,128]{2,1,0:T(8,128)(2,1)S(1)} async-done(((bf16[32,64,128]{2,1,0:T(8,128)(2,1)}), bf16[32,64,128]{2,1,0:T(8,128)(2,1)S(1)}, u32[]{:S(2)}, u32[]{:S(2)}) %all-to-all-start.2) | async-done | bytes 524320 | tf_op jit(solution)/shard_map/all_to_all | solution.py:245
  149.6 0.0 copy-start.8
  149.7 0.8 copy-done.8
  150.4 2.1 assemble.1
  152.5 0.0 copy-start.9
  152.5 3.8 %multiply_reduce_fusion.1 = (f32[256]{0:T(256)S(1)}, f32[256,2048]{1,0:T(8,128)S(1)}) fusion(bf16[256,1024]{1,0:T(8,128)(2,1)} %assemble.1, bf16[1024,2048]{1,0:T(8,128)(2,1)} %param.19), kind=kOutput, calls=%fused_computation.18 | convolution fusion | flops 1074790144 | bytes 6816768 | tf_op jit(solution)/shard_map/dot_general | solution.py:247
  156.3 0.0 copy-done.9
  156.3 0.0 copy-done.10
  156.3 0.0 copy-start.15
  156.3 0.4 add_convert_fusion
  156.7 0.3 fusion
  157.0 0.0 copy-done.15
  157.0 1.2 convolution_convert_fusion.1
  158.2 0.0 copy-start.14
  158.3 73.9 %all_to_all.25 = bf16[32,24,2048]{2,1,0:T(8,128)(2,1)S(1)} all-to-all(bf16[32,24,2048]{2,1,0:T(8,128)(2,1)S(1)} %bitcast.47), channel_id=1, replica_groups=mesh['sp'=8,'tp'=4] {'sp','tp'}, dimensions={0} | all-to-all | bytes 6291456 | tf_op jit(solution)/shard_map/all_to_all | solution.py:267
  232.2 1.7 copy-done.7
  233.9 0.0 copy-done.14
  233.9 3.0 fusion.7
  236.8 0.0 copy-done
  236.8 8.1 %convolution_convert_fusion = bf16[768,2048]{1,0:T(8,128)(2,1)} fusion(bf16[1,512,2048]{2,1,0:T(8,128)(2,1)S(1)} %copy-done, f32[768,512]{1,0:T(8,128)} %fusion.7, bf16[768,2048]{1,0:T(8,128)(2,1)} %bitcast.46, bf16[1,2048,512]{2,1,0:T(8,128)(2,1)} %param.26), kind=kOutput, calls=%fused_computation | convolution fusion | flops 3225157632 | bytes 12058624 | tf_op jit(solution)/shard_map/dot_general | solution.py:272
  245.0 3.8 %all-to-all-start.4 = ((bf16[32,24,2048]{2,1,0:T(8,128)(2,1)}), bf16[32,24,2048]{2,1,0:T(8,128)(2,1)}, u32[]{:S(2)}, u32[]{:S(2)}) async-start(bf16[32,24,2048]{2,1,0:T(8,128)(2,1)} %bitcast.44), calls=%async_computation.4 | async-start | bytes 6291456 | tf_op jit(solution)/shard_map/all_to_all | solution.py:273
  248.8 0.0 copy-done.13
  248.8 71.6 %all-to-all-done.4 = bf16[32,24,2048]{2,1,0:T(8,128)(2,1)} async-done(((bf16[32,24,2048]{2,1,0:T(8,128)(2,1)}), bf16[32,24,2048]{2,1,0:T(8,128)(2,1)}, u32[]{:S(2)}, u32[]{:S(2)}) %all-to-all-start.4) | async-done | bytes 3145760 | tf_op jit(solution)/shard_map/all_to_all | solution.py:273
  320.4 3.0 fusion.22
  323.4 3.1 convolution_add_fusion.1
  326.5 0.0 copy-start.11
  326.5 3.2 multiply_reduce_fusion
  329.8 0.0 copy-done.11
  329.8 1.4 fusion.3
  (15 shorter events, 0.2 us)
Async XLA Ops:
  0.0 236.8 %copy-start = (bf16[1,512,2048]{2,1,0:T(8,128)(2,1)S(1)}, bf16[1,512,2048]{2,1,0:T(8,128)(2,1)}, u32[]{:S(2)}) copy-start(bf16[1,512,2048]{2,1,0:T(8,128)(2,1)} %param.27) | copy-start | bytes 6291460
  0.0 1.2 copy-start.2
  1.2 1.0 copy-start.3
  2.2 1.0 copy-start.4
  4.7 1.2 copy-start.1
  5.9 44.4 %all-to-all-start = ((bf16[8,768,128]{2,1,0:T(8,128)(2,1)}), bf16[8,768,128]{2,1,0:T(8,128)(2,1)}, u32[]{:S(2)}, u32[]{:S(2)}) async-start(bf16[8,768,128]{2,1,0:T(8,128)(2,1)} %copy-done.1), calls=%async_computation | async-start | bytes 3145728 | tf_op jit(solution)/shard_map/all_to_all | solution.py:227
  50.3 36.9 %all-to-all-start.1 = ((bf16[8,512,128]{2,1,0:T(8,128)(2,1)}), bf16[8,512,128]{2,1,0:T(8,128)(2,1)}, u32[]{:S(2)}, u32[]{:S(2)}) async-start(bf16[8,512,128]{2,1,0:T(8,128)(2,1)} %get-tuple-element.12), calls=%async_computation.1 | async-start | bytes 2097152 | tf_op jit(solution)/shard_map/all_to_all | solution.py:229
  56.7 1.9 copy-start.6
  87.2 46.9 %copy-start.12 = (s32[256,2]{0,1:T(2,128)S(1)}, s32[256,2]{0,1:T(2,128)}, u32[]{:S(2)}) copy-start(s32[256,2]{0,1:T(2,128)} %param.23) | copy-start | bytes 6148
  127.3 0.8 copy-start.5
  128.1 21.6 %all-to-all-start.2 = ((bf16[32,64,128]{2,1,0:T(8,128)(2,1)}), bf16[32,64,128]{2,1,0:T(8,128)(2,1)S(1)}, u32[]{:S(2)}, u32[]{:S(2)}) async-start(bf16[32,64,128]{2,1,0:T(8,128)(2,1)} %copy-done.5), calls=%async_computation.2 | async-start | bytes 1048576 | tf_op jit(solution)/shard_map/all_to_all | solution.py:245
  149.6 0.8 copy-start.8
  152.5 3.8 %copy-start.9 = (bf16[256,2048]{1,0:T(8,128)(2,1)S(1)}, bf16[256,2048]{1,0:T(8,128)(2,1)}, u32[]{:S(2)}) copy-start(bf16[256,2048]{1,0:T(8,128)(2,1)} %param.18) | copy-start | bytes 3145732
  152.5 3.8 %copy-start.10 = (f32[2048]{0:T(1024)S(1)}, f32[2048]{0:T(1024)}, u32[]{:S(2)}) copy-start(f32[2048]{0:T(1024)} %param.20) | copy-start | bytes 24580
  156.3 0.7 copy-start.15
  158.2 75.6 %copy-start.14 = (bf16[1,2048,512]{2,1,0:T(8,128)(2,1)S(1)}, bf16[1,2048,512]{2,1,0:T(8,128)(2,1)}, u32[]{:S(2)}) copy-start(bf16[1,2048,512]{2,1,0:T(8,128)(2,1)} %param.25) | copy-start | bytes 6291460
  232.2 1.7 copy-start.7
  245.0 3.8 %copy-start.13 = (f32[256,2]{0,1:T(2,128)S(1)}, f32[256,2]{0,1:T(2,128)}, u32[]{:S(2)}) copy-start(f32[256,2]{0,1:T(2,128)} %param.24) | copy-start | bytes 6148
  245.0 75.4 %all-to-all-start.4 = ((bf16[32,24,2048]{2,1,0:T(8,128)(2,1)}), bf16[32,24,2048]{2,1,0:T(8,128)(2,1)}, u32[]{:S(2)}, u32[]{:S(2)}) async-start(bf16[32,24,2048]{2,1,0:T(8,128)(2,1)} %bitcast.44), calls=%async_computation.4 | async-start | bytes 6291456 | tf_op jit(solution)/shard_map/all_to_all | solution.py:273
  326.5 3.3 copy-start.11

commit v3 on v2

--- a/solution.py
+++ b/solution.py
@@ -140,7 +140,8 @@
 
     if begun:
         before = state_ref[...]
-        state = (before[:, 1:2], jnp.where(out_lane == 1, 0.0, before))
+        kept = jnp.max(jnp.where(out_lane == 1, before, -jnp.inf), axis=1, keepdims=True)
+        state = (kept, jnp.where(out_lane == 1, 0.0, before))
     else:
         state = (
             jnp.full((rows, 1), MASKED, jnp.float32),
@@ -234,11 +235,17 @@
     gate_q = lax.dynamic_index_in_dim(gate_q, me % shares, 1, keepdims=False).reshape(-1)
     ones_q = jnp.ones((n_sp * chunk,), jnp.bfloat16)
     ones_k = jnp.ones((n_sp * tok_dev,), jnp.bfloat16)
-    side_q = jnp.stack(bf16_parts(gate_q) + [ones_q] * 3, axis=1)
-    side_k = jnp.stack([ones_k] * 3 + bf16_parts(-gate), axis=1)
-    pad = ((0, 0), (HEAD_DIM, HEAD_DIM - 6))
-    side_q = jnp.pad(side_q, pad)
-    side_k = jnp.pad(side_k, pad).reshape(n_sp, tok_dev, 2 * HEAD_DIM)
+    lanes = jnp.arange(2 * HEAD_DIM)
+    place_side = (lanes == HEAD_DIM + jnp.arange(6)[:, None]).astype(jnp.bfloat16)
+
+    def side_lanes(parts):
+        return lax.dot_general(
+            jnp.stack(parts), place_side, (((0,), (0,)), ((), ())), preferred_element_type=jnp.float32
+        ).astype(jnp.bfloat16)
+
+    side_q = side_lanes(bf16_parts(gate_q) + [ones_q] * 3)
+    side_k = side_lanes([ones_k] * 3 + bf16_parts(-gate))
+    side_k = side_k.reshape(n_sp, tok_dev, 2 * HEAD_DIM)
     fixed = (first, sub, rows_dev, n_tp, shares)
     state = flash(got, got, side_q, side_k, None, (0, first), *fixed)
     out = flash(got, got_two, side_q, side_k, state, (first, tok_dev), *fixed)

time: 332 us -> 317 us (0.955)
  Pallas kernels: 70 us -> 57.2 us
  local copies, waits for them, and re-layouts: 15.9 us -> 9.91 us
    pallas_call x2, Pallas kernels: 66.6 us -> 53.7 us  [flash(): pl.pallas_call(body, grid=(n_sp,), out_shape=out_shape, in_specs=[q_spec,...]
    pad x2 -> x0, local copies, waits for them, and re-layouts: 3.82 us -> none  [the longest x1 2.06 us: local(): side_k = jnp.pad(side_k, pad).reshape(n_sp, tok_dev, 2 * HEAD_DIM)]
    unnamed x34 -> x35, local copies, waits for them, and re-layouts: 9.89 us -> 9.11 us
  transfers between devices with their start and end apart: 4 -> 4, of which waited for: 3 -> 3; matrix products, arithmetic and copies ran while one was open for 3% -> 2% of each run, Pallas kernels for 8% -> 8%
where the time goes in v3:
time: 317 us; the launch traced here: 316 us
  waiting for transfers between devices  122 us (38%)
  blocking collectives  73.9 us (23%)
  Pallas kernels  57.2 us (18%)
  matrix products  28.2 us (9%)
  starting transfers between devices  20.8 us (7%)
  local copies, waits for them, and re-layouts  9.91 us (3%)
  other arithmetic  3.4 us (1%)
    all_to_all x1, blocking collectives, local(): lax.all_to_all(outgoing, ('sp', 'tp'), split_axis=0, concat_axis=0, tiled...  73.9 us
    all_to_all x1, waiting for transfers between devices, local(): lax.all_to_all(expert_out.reshape(experts_all, capacity, -1), ('sp', 'tp'...  71.6 us
    pallas_call x2, Pallas kernels, flash(): pl.pallas_call(body, grid=(n_sp,), out_shape=out_shape, in_specs=[q_spec,...  53.7 us
    all_to_all x1, waiting for transfers between devices, local(): got = lax.all_to_all(one, 'sp', split_axis=0, concat_axis=0, tiled=True)  36.1 us
    all_to_all x1, waiting for transfers between devices, local(): lax.all_to_all(out, ('sp', 'tp'), split_axis=0, concat_axis=0, tiled=True)  14.8 us
    dot_general x3, matrix products, local(): jnp.dot(part, returned, preferred_element_type=jnp.float32)  9.37 us
    unnamed x35, local copies, waits for them, and re-layouts  9.11 us
    dot_general x1, matrix products, local(): jnp.dot(hidden, w_down[0], preferred_element_type=jnp.float32)  8.12 us
  transfers between devices with their start and end apart: 4, of which 3 were waited for; matrix products, arithmetic and copies ran while one was open for 2% of the time, Pallas kernels for 8%

profile of v3, /device:TPU:0, one launch (start us, length us, event | category | flops | bytes accessed | tf_op | source)
XLA Modules:
  0.0 316.2 jit_solution(4033443789800401812)
XLA Ops:
  0.0 0.0 copy-start
  0.0 0.0 copy-start.4
  0.0 1.2 copy-done.4
  1.2 0.0 copy-start.5
  1.2 1.0 copy-done.5
  2.2 0.0 copy-start.6
  2.2 1.0 copy-done.6
  3.3 1.4 pack.1
  4.7 0.0 copy-start.1
  4.7 1.2 copy-done.1
  5.9 7.3 %all-to-all-start = ((bf16[8,768,128]{2,1,0:T(8,128)(2,1)}), bf16[8,768,128]{2,1,0:T(8,128)(2,1)}, u32[]{:S(2)}, u32[]{:S(2)}) async-start(bf16[8,768,128]{2,1,0:T(8,128)(2,1)} %copy-done.1), calls=%async_computation | async-start | bytes 3145728 | tf_op jit(solution)/shard_map/all_to_all | solution.py:228
  13.1 1.0 fusion.44
  14.2 36.1 %all-to-all-done.refs_0_.refs_1_ = bf16[8,768,128]{2,1,0:T(8,128)(2,1)} async-done(((bf16[8,768,128]{2,1,0:T(8,128)(2,1)}), bf16[8,768,128]{2,1,0:T(8,128)(2,1)}, u32[]{:S(2)}, u32[]{:S(2)}) %all-to-all-start) | async-done | bytes 1572896 | tf_op jit(solution)/shard_map/all_to_all | solution.py:228
  50.2 3.6 %all-to-all-start.1 = ((bf16[8,512,128]{2,1,0:T(8,128)(2,1)}), bf16[8,512,128]{2,1,0:T(8,128)(2,1)S(1)}, u32[]{:S(2)}, u32[]{:S(2)}) async-start(bf16[8,512,128]{2,1,0:T(8,128)(2,1)} %get-tuple-element.12), calls=%async_computation.1 | async-start | bytes 2097152 | tf_op jit(solution)/shard_map/all_to_all | solution.py:230
  54.0 0.1 stack.9
  54.2 0.2 stack.21
  54.4 0.5 convolution_convert_fusion.1.refs_2_
  54.9 0.0 copy-start.2
  55.0 2.3 convolution_convert_fusion
  57.2 0.0 copy-done.2
  57.2 26.4 %flash.2.refs_4_ = f32[4096,128]{1,0:T(8,128)} custom-call(bf16[8,768,128]{2,1,0:T(8,128)(2,1)} %all-to-all-done.refs_0_.refs_1_, bf16[8,768,128]{2,1,0:T(8,128)(2,1)} %all-to-all-done.refs_0_.refs_1_, bf16[4096,128]{1,0:T(8,128)(2,1)S(1)} %convolution_convert_fusion.1.refs_2_, bf16[8,1024,128]{2,1,0:T(8,128)(2,1)} %bitcast.43), custom_call_target="tpu_custom_call" | custom-call | flops 9663676416 | bytes 4194304 | tf_op jit(solution)/shard_map/flash/pallas_call | solution.py:187
  83.7 0.0 all-to-all-done.1.refs_1_
  83.7 0.0 copy-start.3
  83.7 1.2 copy-done.3
  84.9 0.0 copy-start.13
  84.9 27.3 %flash.3 = bf16[32,64,128]{2,1,0:T(8,128)(2,1)S(1)} custom-call(bf16[8,768,128]{2,1,0:T(8,128)(2,1)} %all-to-all-done.refs_0_.refs_1_, bf16[8,512,128]{2,1,0:T(8,128)(2,1)S(1)} %all-to-all-done.1.refs_1_, bf16[4096,128]{1,0:T(8,128)(2,1)S(1)} %copy-done.3, bf16[8,1024,128]{2,1,0:T(8,128)(2,1)} %bitcast.44, f32[4096,128]{1,0:T(8,128)} %flash.2.refs_4_), custom_call_target="tpu_custom_call" | custom-call | flops 9663676416 | bytes 4194304 | tf_op jit(solution)/shard_map/flash/pallas_call | solution.py:187
  112.2 0.0 copy-start.7
  112.2 0.8 copy-done.7
  113.0 6.0 %all-to-all-start.2 = ((bf16[32,64,128]{2,1,0:T(8,128)(2,1)}), bf16[32,64,128]{2,1,0:T(8,128)(2,1)S(1)}, u32[]{:S(2)}, u32[]{:S(2)}) async-start(bf16[32,64,128]{2,1,0:T(8,128)(2,1)} %copy-done.7), calls=%async_computation.2 | async-start | bytes 1048576 | tf_op jit(solution)/shard_map/all_to_all | solution.py:252
  119.0 0.0 copy-done.13
  119.0 0.1 copy.24
  119.2 0.1 eq.41
  119.3 0.3 convert_reduce_fusion
  119.6 0.1 reduce_sum.40
  119.7 0.1 copy.25
  119.8 14.8 %all-to-all-done.2.in_ref = bf16[32,64,128]{2,1,0:T(8,128)(2,1)S(1)} async-done(((bf16[32,64,128]{2,1,0:T(8,128)(2,1)}), bf16[32,64,128]{2,1,0:T(8,128)(2,1)S(1)}, u32[]{:S(2)}, u32[]{:S(2)}) %all-to-all-start.2) | async-done | bytes 524320 | tf_op jit(solution)/shard_map/all_to_all | solution.py:252
  134.6 0.0 copy-start.9
  134.7 0.8 copy-done.9
  135.4 2.1 assemble.1
  137.5 0.0 copy-start.10
  137.5 3.8 %multiply_reduce_fusion.1 = (f32[256]{0:T(256)S(1)}, f32[256,2048]{1,0:T(8,128)S(1)}) fusion(bf16[256,1024]{1,0:T(8,128)(2,1)} %assemble.1, bf16[1024,2048]{1,0:T(8,128)(2,1)} %param.19), kind=kOutput, calls=%fused_computation.20 | convolution fusion | flops 1074790144 | bytes 6816768 | tf_op jit(solution)/shard_map/dot_general | solution.py:254
  141.3 0.0 copy-done.10
  141.3 0.0 copy-done.11
  141.3 0.0 copy-start.16
  141.3 0.4 add_convert_fusion
  141.7 0.3 fusion
  142.0 0.0 copy-done.16
  142.0 1.2 convolution_convert_fusion.3
  143.3 0.0 copy-start.15
  143.3 73.9 %all_to_all.25 = bf16[32,24,2048]{2,1,0:T(8,128)(2,1)S(1)} all-to-all(bf16[32,24,2048]{2,1,0:T(8,128)(2,1)S(1)} %bitcast.42), channel_id=1, replica_groups=mesh['sp'=8,'tp'=4] {'sp','tp'}, dimensions={0} | all-to-all | bytes 6291456 | tf_op jit(solution)/shard_map/all_to_all | solution.py:274
  217.2 1.7 copy-done.8
  218.9 0.0 copy-done.15
  218.9 3.0 fusion.7
  221.8 0.0 copy-done
  221.8 8.1 %convolution_convert_fusion.2 = bf16[768,2048]{1,0:T(8,128)(2,1)} fusion(bf16[1,512,2048]{2,1,0:T(8,128)(2,1)S(1)} %copy-done, f32[768,512]{1,0:T(8,128)} %fusion.7, bf16[768,2048]{1,0:T(8,128)(2,1)} %bitcast.41, bf16[1,2048,512]{2,1,0:T(8,128)(2,1)} %param.26), kind=kOutput, calls=%fused_computation.2 | convolution fusion | flops 3225157632 | bytes 12058624 | tf_op jit(solution)/shard_map/dot_general | solution.py:279
  230.0 3.8 %all-to-all-start.4 = ((bf16[32,24,2048]{2,1,0:T(8,128)(2,1)}), bf16[32,24,2048]{2,1,0:T(8,128)(2,1)}, u32[]{:S(2)}, u32[]{:S(2)}) async-start(bf16[32,24,2048]{2,1,0:T(8,128)(2,1)} %bitcast.39), calls=%async_computation.4 | async-start | bytes 6291456 | tf_op jit(solution)/shard_map/all_to_all | solution.py:280
  233.8 0.0 copy-done.14
  233.8 71.6 %all-to-all-done.4 = bf16[32,24,2048]{2,1,0:T(8,128)(2,1)} async-done(((bf16[32,24,2048]{2,1,0:T(8,128)(2,1)}), bf16[32,24,2048]{2,1,0:T(8,128)(2,1)}, u32[]{:S(2)}, u32[]{:S(2)}) %all-to-all-start.4) | async-done | bytes 3145760 | tf_op jit(solution)/shard_map/all_to_all | solution.py:280
  305.4 3.0 fusion.22
  308.4 3.1 convolution_add_fusion.1
  311.5 0.0 copy-start.12
  311.5 3.2 %multiply_reduce_fusion = (f32[256]{0:T(256)S(1)}, f32[256,2048]{1,0:T(8,128)S(1)}) fusion(f32[256,2048]{1,0:T(8,128)S(1)} %convolution_add_fusion.1, bf16[768,2048]{1,0:T(8,128)(2,1)} %bitcast.13, f32[256]{0:T(256)S(1)} %bitcast.59, s32[256]{0:T(256)S(1)} %bitcast.53, f32[256]{0:T(256)S(1)} %bitcast.56, s32[256]{0:T(256)S(1)} %bitcast.49), kind=kOutput, calls=%fused_computation.18 | convolution fusion | flops 809041664 | bytes 7345152 | tf_op jit(solution)/shard_map/dot_general | solution.py:292
  314.8 0.0 copy-done.12
  314.8 1.4 fusion.3
  (16 shorter events, 0.2 us)
Async XLA Ops:
  0.0 221.8 %copy-start = (bf16[1,512,2048]{2,1,0:T(8,128)(2,1)S(1)}, bf16[1,512,2048]{2,1,0:T(8,128)(2,1)}, u32[]{:S(2)}) copy-start(bf16[1,512,2048]{2,1,0:T(8,128)(2,1)} %param.27) | copy-start | bytes 6291460
  0.0 1.2 copy-start.4
  1.2 1.0 copy-start.5
  2.2 1.0 copy-start.6
  4.7 1.2 copy-start.1
  5.9 44.4 %all-to-all-start = ((bf16[8,768,128]{2,1,0:T(8,128)(2,1)}), bf16[8,768,128]{2,1,0:T(8,128)(2,1)}, u32[]{:S(2)}, u32[]{:S(2)}) async-start(bf16[8,768,128]{2,1,0:T(8,128)(2,1)} %copy-done.1), calls=%async_computation | async-start | bytes 3145728 | tf_op jit(solution)/shard_map/all_to_all | solution.py:228
  50.2 33.4 %all-to-all-start.1 = ((bf16[8,512,128]{2,1,0:T(8,128)(2,1)}), bf16[8,512,128]{2,1,0:T(8,128)(2,1)S(1)}, u32[]{:S(2)}, u32[]{:S(2)}) async-start(bf16[8,512,128]{2,1,0:T(8,128)(2,1)} %get-tuple-element.12), calls=%async_computation.1 | async-start | bytes 2097152 | tf_op jit(solution)/shard_map/all_to_all | solution.py:230
  54.9 2.3 copy-start.2
  83.7 1.2 copy-start.3
  84.9 34.1 %copy-start.13 = (s32[256,2]{0,1:T(2,128)S(1)}, s32[256,2]{0,1:T(2,128)}, u32[]{:S(2)}) copy-start(s32[256,2]{0,1:T(2,128)} %param.23) | copy-start | bytes 6148
  112.2 0.8 copy-start.7
  113.0 21.7 %all-to-all-start.2 = ((bf16[32,64,128]{2,1,0:T(8,128)(2,1)}), bf16[32,64,128]{2,1,0:T(8,128)(2,1)S(1)}, u32[]{:S(2)}, u32[]{:S(2)}) async-start(bf16[32,64,128]{2,1,0:T(8,128)(2,1)} %copy-done.7), calls=%async_computation.2 | async-start | bytes 1048576 | tf_op jit(solution)/shard_map/all_to_all | solution.py:252
  134.6 0.8 copy-start.9
  137.5 3.8 %copy-start.10 = (bf16[256,2048]{1,0:T(8,128)(2,1)S(1)}, bf16[256,2048]{1,0:T(8,128)(2,1)}, u32[]{:S(2)}) copy-start(bf16[256,2048]{1,0:T(8,128)(2,1)} %param.18) | copy-start | bytes 3145732
  137.5 3.8 %copy-start.11 = (f32[2048]{0:T(1024)S(1)}, f32[2048]{0:T(1024)}, u32[]{:S(2)}) copy-start(f32[2048]{0:T(1024)} %param.20) | copy-start | bytes 24580
  141.3 0.7 copy-start.16
  143.3 75.6 %copy-start.15 = (bf16[1,2048,512]{2,1,0:T(8,128)(2,1)S(1)}, bf16[1,2048,512]{2,1,0:T(8,128)(2,1)}, u32[]{:S(2)}) copy-start(bf16[1,2048,512]{2,1,0:T(8,128)(2,1)} %param.25) | copy-start | bytes 6291460
  217.2 1.7 copy-start.8
  230.0 3.8 %copy-start.14 = (f32[256,2]{0,1:T(2,128)S(1)}, f32[256,2]{0,1:T(2,128)}, u32[]{:S(2)}) copy-start(f32[256,2]{0,1:T(2,128)} %param.24) | copy-start | bytes 6148
  230.0 75.4 %all-to-all-start.4 = ((bf16[32,24,2048]{2,1,0:T(8,128)(2,1)}), bf16[32,24,2048]{2,1,0:T(8,128)(2,1)}, u32[]{:S(2)}, u32[]{:S(2)}) async-start(bf16[32,24,2048]{2,1,0:T(8,128)(2,1)} %bitcast.39), calls=%async_computation.4 | async-start | bytes 6291456 | tf_op jit(solution)/shard_map/all_to_all | solution.py:280
  311.5 3.3 %copy-start.12 = (f32[2048]{0:T(1024)S(1)}, f32[2048]{0:T(1024)}, u32[]{:S(2)}) copy-start(f32[2048]{0:T(1024)} %param.22) | copy-start | bytes 24580
